TPU v7x, 512 devices: a whole 4x4x16 slice. The times are simulated.
512 devices in a mesh: sp: 64 (over z, y), tp: 8 (over x, core).
Axes of the slice: x: 4, y: 4, z: 16, core: 2. Of those that a mesh axis runs over, the one named last changes fastest.
Arguments:
- tokens: bfloat16 [16384, 2048], P('sp'), may hold values from -6 to 6
- ln_gain: float32 [2048], replicated, may hold values from 0.1 to 1.9
- w_query_attn: bfloat16 [2048, 1024], P('sp', 'tp'), may hold values from -0.125 to 0.125
- w_key_attn: bfloat16 [2048, 1024], P('sp', 'tp'), may hold values from -0.125 to 0.125
- w_value_attn: bfloat16 [2048, 1024], P('sp', 'tp'), may hold values from -0.125 to 0.125
- w_query_delta: bfloat16 [2048, 1024], P('sp', 'tp'), may hold values from -0.125 to 0.125
- w_key_delta: bfloat16 [2048, 1024], P('sp', 'tp'), may hold values from -0.125 to 0.125
- w_value_delta: bfloat16 [2048, 1024], P('sp', 'tp'), may hold values from -0.125 to 0.125
- w_beta: bfloat16 [2048, 8], replicated, may hold values from -0.125 to 0.125
- w_decay: bfloat16 [2048, 8], replicated, may hold values from -0.125 to 0.125
- attn_bias: float32 [16], replicated, may hold values from -13 to 1
- decay_log: float32 [8], replicated, may hold values from -15 to -2
- beta_bias: float32 [8], replicated, may hold values from -7 to 1
- log_decay_extra: float32 [16384, 8], P('sp', 'tp'), may hold values from -0.7 to 0, as said below
- attn_gain: float32 [64], replicated, may hold values from 0.1 to 1.9
- delta_gain: float32 [128], replicated, may hold values from 0.1 to 1.9
- w_out_attn: bfloat16 [1024, 2048], P('tp', 'sp'), may hold values from -0.125 to 0.125
- w_out_delta: bfloat16 [1024, 2048], P('tp', 'sp'), may hold values from -0.125 to 0.125
Outputs:
- mixed_out: bfloat16 [16384, 2048], P(('sp', 'tp'))
Inputs may be any that keep to these rules, and one draw needn't show every extreme that they name: `log_decay_extra`: never positive.
All inputs are finite; a program needn't handle non-finite values.
Results may differ from a plain program's by a relative error of at most 0.015.
Values may be sent and summed in bfloat16 or wider, within the bound.
A program may use at most 128 MiB of HBM per device.

v0:
```python
import math
import jax
import jax.numpy as jnp
from jax import lax
from jax.sharding import Mesh
from jax.sharding import PartitionSpec as P

SB_DIM = 64
GDN_DIM = 128
DBLOCK = 64
SP = ("sp_0", "sp_1")
SP_TP = ("sp_0", "sp_1", "tp")


def side_by_side(arrays, axis, dim, along):
    widths = [a.shape[along] for a in arrays]
    both = jnp.concatenate(arrays, axis=along)
    result = lax.all_gather(both, axis, axis=dim, tiled=True)
    return tuple(jnp.split(result, [sum(widths[:k]) for k in range(1, len(widths))], axis=along))


def neutral_like(value, identity):
    return jax.tree.map(
        lambda a, e: jnp.broadcast_to(jnp.asarray(e, a.dtype), a.shape), value, identity
    )


def carried_in(value, axes, combine, identity):
    before = start = neutral_like(value, identity)
    running = value
    for axis in reversed(axes):
        length, index = (lax.axis_size(axis), lax.axis_index(axis))
        pieces = jax.tree.map(lambda part: lax.all_gather(part, axis), running)
        inside, running = (start, start)
        for k in range(length):
            passed = k < index
            running = combine(running, jax.tree.map(lambda part: part[k], pieces))
            inside = jax.tree.map(lambda new, old: jnp.where(passed, new, old), running, inside)
        before = combine(inside, before)
    return before


def turned_gather(arrays, axis, dims):
    turned = [jnp.moveaxis(a, dim, 0) for a, dim in zip(arrays, dims)]
    widths = [t[0].size for t in turned]
    both = jnp.concatenate([t.reshape(-1, w) for t, w in zip(turned, widths)], axis=1)
    result = lax.all_gather(both, axis, axis=0, tiled=True)
    pieces = jnp.split(result, [sum(widths[:k]) for k in range(1, len(widths))], axis=1)
    return tuple(
        (
            jnp.moveaxis(b.reshape(-1, *t.shape[1:]), 0, dim)
            for b, t, dim in zip(pieces, turned, dims)
        )
    )


def cut_along(value, dim, length):
    before, after = (value.shape[:dim], value.shape[dim + 1 :])
    return jnp.moveaxis(value.reshape(*before, length, -1, *after), dim, 0)


def summed_on_arrival(value, axis, dim):
    length = lax.axis_size(axis)
    pieces = lax.all_to_all(cut_along(value, dim, length), axis, 0, 0, tiled=True)
    return jnp.sum(pieces.astype(jnp.float32), axis=0)


def layer_normed(tok_rows, ln_gain):
    values = tok_rows.astype(jnp.float32)
    center = jnp.mean(values, axis=-1, keepdims=True)
    spread = jnp.mean(jnp.square(values - center), axis=-1, keepdims=True)
    return ((values - center) * lax.rsqrt(spread + 1e-05) * ln_gain).astype(jnp.bfloat16)


def rms_scaled(values, gain):
    return values * lax.rsqrt(jnp.mean(jnp.square(values), axis=-1, keepdims=True) + 1e-06) * gain


def unit_rows(values):
    return values * lax.rsqrt(jnp.sum(jnp.square(values), axis=-1, keepdims=True) + 1e-06)


def stick_block(carry, queries, query_pos, head_bias, key_block, value_block, key_first):
    outputs, log_kept = carry
    key_count = key_block.shape[0]
    heads = queries.shape[1]
    head_width = queries.shape[2]
    scores = jnp.einsum(
        "rhd,khd->hrk",
        queries,
        key_block.reshape(key_count, heads, head_width),
        preferred_element_type=jnp.float32,
    )
    scores = scores * head_width ** (-0.5) + head_bias[:, None, None]
    key_pos = key_first + jnp.arange(key_count, dtype=jnp.int32)
    visible = (key_pos[None, :] < query_pos[:, None]) & (key_pos[None, :] >= 0)
    lost = jnp.where(visible[None], -jax.nn.softplus(scores), 0.0)
    between = lax.cumsum(lost, axis=2, reverse=True) - lost + log_kept[:, :, None]
    weights = jnp.where(visible[None], jnp.exp(jax.nn.log_sigmoid(scores) + between), 0.0).astype(
        jnp.bfloat16
    )
    outputs = outputs + jnp.einsum(
        "hrk,khd->hrd",
        weights,
        value_block.reshape(key_count, heads, head_width),
        preferred_element_type=jnp.float32,
    )
    return (outputs, log_kept + jnp.sum(lost, axis=2))


def stick_span(carry, queries, query_pos, head_bias, keys, values, key_first):
    own_rows = queries.shape[0]
    length = keys.shape[0]
    widest = max(1, 1024 // own_rows)
    widest = 1 << widest.bit_length() - 1
    block = own_rows * math.gcd(widest, length // own_rows)
    blocks = length // block

    def one_turn(step_index, inner):
        block_index = blocks - 1 - step_index
        key_block = lax.dynamic_slice_in_dim(keys, block_index * block, block, 0)
        value_block = lax.dynamic_slice_in_dim(values, block_index * block, block, 0)
        return stick_block(
            inner,
            queries,
            query_pos,
            head_bias,
            key_block,
            value_block,
            key_first + block_index * block,
        )

    return lax.fori_loop(0, blocks, one_turn, carry)


def delta_parts(queries, keys, values, beta, decay):
    width = queries.shape[-2]
    key_width = queries.shape[-1]
    decay_sum = jnp.cumsum(decay, axis=-1)
    lower = jnp.tril(jnp.ones((width, width), dtype=bool))
    strict = jnp.tril(jnp.ones((width, width), dtype=bool), -1)
    differ = decay_sum[..., :, None] - decay_sum[..., None, :]
    decay_mask = jnp.where(lower, jnp.exp(jnp.where(lower, differ, 0.0)), 0.0)
    keys_beta = keys * beta[..., None]
    values_beta = values * beta[..., None]
    strict_mat = jnp.where(
        strict, jnp.einsum("...id,...jd->...ij", keys_beta, keys) * decay_mask, 0.0
    )
    right_side = jnp.concatenate([keys_beta * jnp.exp(decay_sum)[..., None], values_beta], axis=-1)
    solved = jax.scipy.linalg.solve_triangular(
        jnp.eye(width, dtype=jnp.float32) + strict_mat, right_side, lower=True
    )
    solve_keys = solved[..., :key_width]
    solve_values = solved[..., key_width:]
    query_key = jnp.einsum("...id,...jd->...ij", queries, keys) * decay_mask
    query_decayed = queries * jnp.exp(decay_sum)[..., None]
    keys_to_end = keys * jnp.exp(decay_sum[..., -1:] - decay_sum)[..., None]
    block_decay = jnp.exp(decay_sum[..., -1])
    return (solve_keys, solve_values, query_decayed, query_key, keys_to_end, block_decay)


def delta_update(state, block_parts):
    solve_keys, solve_values, query_decayed, query_key, keys_to_end, block_decay = block_parts
    fresh = solve_values - jnp.einsum("hcd,hde->hce", solve_keys, state)
    outputs = jnp.einsum("hcd,hde->hce", query_decayed, state)
    outputs = outputs + jnp.einsum("hij,hje->hie", query_key, fresh)
    state = state * block_decay[:, None, None] + jnp.einsum("hcd,hce->hde", keys_to_end, fresh)
    return (state, outputs)


def chain_combine(earlier, later):
    earlier_map, earlier_state = earlier
    later_map, later_state = later
    joined_map = jnp.einsum("hij,hjk->hik", later_map, earlier_map)
    joined_state = jnp.einsum("hij,hjk->hik", later_map, earlier_state) + later_state
    return (joined_map, joined_state)


def local(
    tokens,
    ln_gain,
    w_query_attn,
    w_key_attn,
    w_value_attn,
    w_query_delta,
    w_key_delta,
    w_value_delta,
    w_beta,
    w_decay,
    attn_bias,
    decay_log,
    beta_bias,
    log_decay_extra,
    attn_gain,
    delta_gain,
    w_out_attn,
    w_out_delta,
):
    row_count = tokens.shape[0]
    normed = layer_normed(tokens, ln_gain)
    segments = side_by_side(
        (w_query_attn, w_key_attn, w_value_attn, w_query_delta, w_key_delta, w_value_delta),
        SP,
        0,
        1,
    )
    summed = tuple(
        (jnp.dot(normed, segment, preferred_element_type=jnp.float32) for segment in segments)
    )
    attn_query, attn_key, attn_value, delta_query, delta_key, delta_value = [
        result.astype(jnp.bfloat16) for result in summed
    ]
    tp_pos = lax.axis_index("tp")
    sp_pos = lax.axis_index(SP)
    attn_heads = attn_query.shape[1] // SB_DIM
    delta_heads = delta_query.shape[1] // GDN_DIM
    positions = sp_pos * row_count + jnp.arange(row_count, dtype=jnp.int32)
    queries = attn_query.reshape(row_count, attn_heads, SB_DIM)
    head_bias = lax.dynamic_slice_in_dim(attn_bias, tp_pos * attn_heads, attn_heads, 0)
    carry = (
        jnp.zeros((attn_heads, row_count, SB_DIM), jnp.float32),
        jnp.zeros((attn_heads, row_count), jnp.float32),
    )
    every_key, every_value = side_by_side((attn_key, attn_value), SP, 0, 1)
    carry = stick_span(carry, queries, positions, head_bias, every_key, every_value, 0)
    attn_mixed = rms_scaled(carry[0], attn_gain).astype(jnp.bfloat16)
    head_first = tp_pos * delta_heads
    beta_cols = lax.dynamic_slice_in_dim(w_beta, head_first, delta_heads, 1)
    decay_cols = lax.dynamic_slice_in_dim(w_decay, head_first, delta_heads, 1)
    beta_pre = jnp.dot(normed, beta_cols, preferred_element_type=jnp.float32).astype(jnp.bfloat16)
    decay_pre = jnp.dot(normed, decay_cols, preferred_element_type=jnp.float32).astype(jnp.bfloat16)
    queries = unit_rows(
        jax.nn.silu(delta_query.astype(jnp.float32)).reshape(row_count, delta_heads, GDN_DIM)
    ) * GDN_DIM ** (-0.5)
    keys = unit_rows(
        jax.nn.silu(delta_key.astype(jnp.float32)).reshape(row_count, delta_heads, GDN_DIM)
    )
    values = jax.nn.silu(delta_value.astype(jnp.float32)).reshape(row_count, delta_heads, GDN_DIM)
    beta = jax.nn.sigmoid(
        beta_pre.astype(jnp.float32)
        + lax.dynamic_slice_in_dim(beta_bias, head_first, delta_heads, 0)
    )
    rates = jnp.exp(lax.dynamic_slice_in_dim(decay_log, head_first, delta_heads, 0))
    decay = -rates * jax.nn.softplus(decay_pre.astype(jnp.float32)) + log_decay_extra
    blocks = row_count // DBLOCK

    def to_blocks(array):
        return jnp.moveaxis(array.reshape((blocks, DBLOCK) + array.shape[1:]), 2, 0)

    parts = delta_parts(
        to_blocks(queries), to_blocks(keys), to_blocks(values), to_blocks(beta), to_blocks(decay)
    )
    sequence = tuple((jnp.moveaxis(piece_part, 1, 0) for piece_part in parts))
    eye_mat = jnp.eye(GDN_DIM, dtype=jnp.float32)

    def carry_map(accum, block_parts):
        transition, written = accum
        solve_keys, solve_values, query_decayed, query_key, keys_to_end, block_decay = block_parts
        step_matrix = block_decay[:, None, None] * eye_mat - jnp.einsum(
            "hcd,hce->hde", keys_to_end, solve_keys
        )
        transition = jnp.einsum("hij,hjk->hik", step_matrix, transition)
        written = jnp.einsum("hij,hjk->hik", step_matrix, written)
        written = written + jnp.einsum("hcd,hce->hde", keys_to_end, solve_values)
        return ((transition, written), None)

    neutral = (
        jnp.broadcast_to(eye_mat, (delta_heads, GDN_DIM, GDN_DIM)),
        jnp.zeros((delta_heads, GDN_DIM, GDN_DIM), jnp.float32),
    )
    own_chain, _ = lax.scan(carry_map, neutral, sequence)
    _, incoming = carried_in(own_chain, SP, chain_combine, neutral)
    _, outputs = lax.scan(delta_update, incoming, sequence)
    delta_raw = jnp.moveaxis(outputs, 0, 1).reshape(delta_heads, row_count, GDN_DIM)
    delta_mixed = rms_scaled(delta_raw, delta_gain).astype(jnp.bfloat16)
    full_attn, full_delta = turned_gather((w_out_attn, w_out_delta), SP, (1, 1))
    attn_weight3 = full_attn.reshape(attn_heads, SB_DIM, full_attn.shape[1])
    delta_weight3 = full_delta.reshape(delta_heads, GDN_DIM, full_delta.shape[1])
    result = jnp.einsum("hrd,hdn->rn", attn_mixed, attn_weight3, preferred_element_type=jnp.float32)
    mixed_rows = summed_on_arrival(
        (
            result
            + jnp.einsum(
                "hrd,hdn->rn", delta_mixed, delta_weight3, preferred_element_type=jnp.float32
            )
        ).astype(jnp.bfloat16),
        "tp",
        0,
    )
    return mixed_rows.astype(jnp.bfloat16)


def solution(mesh):
    split = Mesh(mesh.devices.reshape(16, 4, mesh.shape["tp"]), ("sp_0", "sp_1", "tp"))
    return jax.shard_map(
        local,
        mesh=split,
        in_specs=(
            P(SP, None),
            P(),
            P(SP, "tp"),
            P(SP, "tp"),
            P(SP, "tp"),
            P(SP, "tp"),
            P(SP, "tp"),
            P(SP, "tp"),
            P(),
            P(),
            P(),
            P(),
            P(),
            P(SP, "tp"),
            P(),
            P(),
            P("tp", SP),
            P("tp", SP),
        ),
        out_specs=P(SP_TP, None),
        check_vma=False,
    )
```

profile of v0, /device:TPU:1, one launch (start us, length us, event | category | flops | bytes accessed | tf_op | source)
XLA Modules:
  0.0 829.6 jit_solution(2809152960668360981)
XLA Ops:
  21.7 129.8 %all-gather.9.cloned.1.call-done = bf16[2048,768]{1,0:T(8,128)(2,1)} async-done(((bf16[32,768]{1,0:T(8,128)(2,1)}), bf16[2048,768]{1,0:T(8,128)(2,1)}) %all-gather.9.cloned.1.call-update) | async-done | bytes 3145744 | tf_op jit(solution)/shard_map/all_gather | solution.py:18
  153.3 19.7 %custom-call.4 = f32[4,1,64,64]{2,3,1,0:T(8,128)S(1)} custom-call(f32[4,1,64,64]{3,2,1,0:T(8,128)S(1)} %fusion.60), custom_call_target="InvertDiagBlocksLowerTriangular" | custom-call | tf_op jit(solution)/shard_map/jit(_solve_triangular)/vmap()/triangular_solve | solution.py:150
  175.2 7.6 while.42
  182.9 9.2 %all-gather = bf16[4,128,128]{2,1,0:T(8,128)(2,1)S(1)} all-gather(bf16[1,128,128]{2,1,0:T(8,128)(2,1)S(1)} %get-tuple-element.235), channel_id=2, replica_groups=mesh['sp_0'=16,'sp_1'=4,'tp'=8] {'sp_1'}, dimensions={0}, use_global_device_ids=true | all-gather | bytes 163840 | tf_op jit(solution)/shard_map/all_gather | solution.py:33
  192.0 9.8 %all-gather.2 = f32[4,128,128]{2,1,0:T(8,128)S(1)} all-gather(f32[1,128,128]{2,1,0:T(8,128)S(1)} %get-tuple-element.236), channel_id=4, replica_groups=mesh['sp_0'=16,'sp_1'=4,'tp'=8] {'sp_1'}, dimensions={0}, use_global_device_ids=true | all-gather | bytes 327680 | tf_op jit(solution)/shard_map/all_gather | solution.py:33
  207.0 81.6 %all-gather.13.cloned.1.call-done = bf16[2048,256]{1,0:T(8,128)(2,1)} async-done(((bf16[32,256]{1,0:T(8,128)(2,1)}), bf16[2048,256]{1,0:T(8,128)(2,1)}) %all-gather.13.cloned.1.call-update) | async-done | bytes 1048592 | tf_op jit(solution)/shard_map/all_gather | solution.py:47
  292.4 23.6 %all-gather.1 = bf16[2048,128]{1,0:T(8,128)(2,1)S(1)} all-gather(bf16[128,128]{1,0:T(8,128)(2,1)S(1)} %fusion.140), channel_id=3, replica_groups=mesh['sp_0'=16,'sp_1'=4,'tp'=8] {'sp_0'}, dimensions={0}, use_global_device_ids=true | all-gather | bytes 557056 | tf_op jit(solution)/shard_map/all_gather | solution.py:33
  317.6 39.7 %all-gather.15.cloned.1.call-done = f32[2048,128]{1,0:T(8,128)} async-done(((f32[128,128]{1,0:T(8,128)}), f32[2048,128]{1,0:T(8,128)}) %all-gather.15.cloned.1.call-update) | async-done | bytes 1048592 | tf_op jit(solution)/shard_map/all_gather | solution.py:33
  373.3 6.9 while.41
  380.5 145.7 %all-gather.11.cloned.1.call-done = bf16[16384,256]{0,1:T(8,128)(2,1)} async-done(((bf16[256,256]{0,1:T(8,128)(2,1)}), bf16[16384,256]{0,1:T(8,128)(2,1)}) %all-gather.11.cloned.1.call-update) | async-done | bytes 8388624 | tf_op jit(solution)/shard_map/all_gather | solution.py:18
  526.2 5.8 fusion.199
  532.0 259.6 %while.43 = (s32[]{:T(128)}, f32[2,256,64]{1,2,0:T(8,128)S(1)}, f32[2,256]{1,0:T(2,128)S(1)}, bf16[16384,128]{0,1:T(8,128)(2,1)}, bf16[256,2,64]{0,2,1:T(8,128)(...) while((s32[]{:T(128)}, f32[2,256,64]{1,2,0:T(8,128)S(1)}, ...), condition=%wide.region_6.7_spmd.clone, body=%wide.region_2.6_spmd.clone.sunk | while | flops 215584000 | bytes 44771616 | solution.py:133
  536.5 5.0 fusion.312
  552.7 5.0 fusion.312
  569.0 5.0 fusion.312
  585.2 5.0 fusion.312
  601.4 5.0 fusion.312
  617.7 5.0 fusion.312
  633.9 5.0 fusion.312
  650.1 5.0 fusion.312
  682.6 5.0 fusion.312
  747.5 5.0 fusion.312
  763.7 5.0 fusion.312
  793.3 28.9 %all_to_all.5 = bf16[8,32,2048]{2,1,0:T(8,128)(2,1)S(1)} all-to-all(bf16[8,32,2048]{2,1,0:T(8,128)(2,1)S(1)} %bitcast.318), channel_id=1, replica_groups=mesh['sp_0'=16,'sp_1'=4,'tp'=8] {'tp'}, dimensions={0} | all-to-all | bytes 2097152 | tf_op jit(solution)/shard_map/all_to_all | solution.py:64
  (457 shorter events, 264.2 us)
Async XLA Ops:
  6.5 11.4 %copy-start = (bf16[2048,8]{0,1:T(8,128)(2,1)S(1)}, bf16[2048,8]{0,1:T(8,128)(2,1)}, u32[]{:S(2)}) copy-start(bf16[2048,8]{0,1:T(8,128)(2,1)} %param.33) | copy-start | bytes 98308
  6.5 11.0 %copy-start.3 = (bf16[256,2048]{1,0:T(8,128)(2,1)S(1)}, bf16[256,2048]{1,0:T(8,128)(2,1)}, u32[]{:S(2)}) copy-start(bf16[256,2048]{1,0:T(8,128)(2,1)} %param.24) | copy-start | bytes 3145732
  6.5 9.6 %copy-start.11 = (f32[8]{0:T(128)S(1)}, f32[8]{0:T(128)}, u32[]{:S(2)}) copy-start(f32[8]{0:T(128)} %param.35) | copy-start | bytes 100
  6.5 11.0 %copy-start.7 = (f32[2048]{0:T(1024)S(1)}, f32[2048]{0:T(1024)}, u32[]{:S(2)}) copy-start(f32[2048]{0:T(1024)} %param.25) | copy-start | bytes 24580
  6.5 144.9 %all-gather.9.cloned.1.call-start = ((), (), s32[]{:S(2)}) async-start(), calls=%async_computation.1 | async-start | bytes 3194880 | tf_op jit(solution)/shard_map/all_gather | solution.py:18
  11.5 277.0 %all-gather.13.cloned.1.call-start = ((), (), s32[]{:S(2)}) async-start(), calls=%async_computation.3 | async-start | bytes 1064960 | tf_op jit(solution)/shard_map/all_gather | solution.py:47
  12.9 344.4 %all-gather.15.cloned.1.call-start = ((), (), s32[]{:S(2)}) async-start(), calls=%async_computation.4 | async-start | bytes 1114112 | tf_op jit(solution)/shard_map/all_gather | solution.py:33
  203.0 323.2 %all-gather.11.cloned.1.call-start = ((), (), s32[]{:S(2)}) async-start(), calls=%async_computation.2 | async-start | bytes 8519680 | tf_op jit(solution)/shard_map/all_gather | solution.py:18
  317.6 55.6 %copy-start.5 = (f32[128,128]{1,0:T(8,128)S(1)}, f32[128,128]{1,0:T(8,128)}, u32[]{:S(2)}) copy-start(f32[128,128]{1,0:T(8,128)} %convolution_add_fusion.20) | copy-start | bytes 196612
  372.0 8.4 %copy-start.9 = (f32[128]{0:T(128)S(1)}, f32[128]{0:T(128)}, u32[]{:S(2)}) copy-start(f32[128]{0:T(128)} %param.39) | copy-start | bytes 1540
  532.0 259.7 %copy-start.10 = (f32[64]{0:T(128)S(1)}, f32[64]{0:T(128)}, u32[]{:S(2)}) copy-start(f32[64]{0:T(128)} %param.38) | copy-start | bytes 772
  536.5 5.0 copy-start.1
  552.7 5.0 copy-start.1
  569.0 5.0 copy-start.1
  585.2 5.0 copy-start.1
  601.4 5.0 copy-start.1
  617.7 5.0 copy-start.1
  633.9 5.0 copy-start.1
  650.1 5.0 copy-start.1
  666.3 5.0 copy-start.1
  682.6 5.0 copy-start.1
  731.2 5.0 copy-start.1
  747.5 5.0 copy-start.1
  763.7 5.0 copy-start.1
  (24 other events, 59.4 us)
Sparse Core Ops, SparseCore 0:
  11.7 139.7 all-gather.8
  154.3 134.1 all-gather.12
  290.6 66.6 all-gather.14
  360.1 166.0 all-gather.10
where the time goes:
time: 832 us; the launch traced here: 830 us
  waiting for transfers between devices  397 us (48%)
  other arithmetic  184 us (22%)
  matrix products  93.2 us (11%)
  blocking collectives  71.5 us (9%)
  local copies, waits for them, and re-layouts  67.3 us (8%)
  between operations  14.3 us (2%)
    all_gather x2, waiting for transfers between devices, side_by_side(): result = lax.all_gather(both, axis, axis=dim, tiled=True)  275 us
    all_gather x1, waiting for transfers between devices, turned_gather(): result = lax.all_gather(both, axis, axis=0, tiled=True)  81.6 us
    another operation x32, other arithmetic  81.2 us
    convert_element_type x16, other arithmetic, stick_block(): jnp.where(visible[None], jnp.exp(jax.nn.log_sigmoid(scores) + between), 0.0)  67.1 us
    dot_general x16, matrix products, stick_block(): jnp.einsum('rhd,khd->hrk', queries, key_block.reshape(key_count, heads, h...  48.4 us
    all_gather x3, blocking collectives, carried_in(): pieces = jax.tree.map(lambda part: lax.all_gather(part, axis), running)  42.6 us
    all_gather x1, waiting for transfers between devices, carried_in(): pieces = jax.tree.map(lambda part: lax.all_gather(part, axis), running)  39.7 us
    another operation x16, local copies, waits for them, and re-layouts, stick_block(): lax.cumsum(lost, axis=2, reverse=True) - lost + log_kept[:, :, None]  30.7 us
  transfers between devices with their start and end apart: 4, of which 4 were waited for; matrix products, arithmetic and copies ran while one was open for 9% of the time, Pallas kernels for 0%

commit v1 on v0

--- a/solution.py
+++ b/solution.py
@@ -44,7 +44,9 @@
     turned = [jnp.moveaxis(a, dim, 0) for a, dim in zip(arrays, dims)]
     widths = [t[0].size for t in turned]
     both = jnp.concatenate([t.reshape(-1, w) for t, w in zip(turned, widths)], axis=1)
-    result = lax.all_gather(both, axis, axis=0, tiled=True)
+    result = jnp.concatenate(
+        lax.all_to_all(jnp.stack([both] * lax.axis_size(axis)), axis, 0, 0), axis=0
+    )
     pieces = jnp.split(result, [sum(widths[:k]) for k in range(1, len(widths))], axis=1)
     return tuple(
         (

time: 832 us -> 773 us (0.929)
  waiting for transfers between devices: 397 us -> 304 us
  matrix products: 93.2 us -> 110 us
    all_gather x1 -> x0, waiting for transfers between devices: 81.6 us -> none  [turned_gather(): result = lax.all_gather(both, axis, axis=0, tiled=True)]
    all_to_all x0 -> x1, waiting for transfers between devices: none -> 41 us  [turned_gather(): lax.all_to_all(jnp.stack([both] * lax.axis_size(axis)), axis, 0, 0)]
    all_gather x1, waiting for transfers between devices: 39.7 us -> 0.02 us  [carried_in(): pieces = jax.tree.map(lambda part: lax.all_gather(part, axis), running)]
    dot_general x16, matrix products: 48.4 us -> 61.5 us  [stick_block(): jnp.einsum('rhd,khd->hrk', queries, key_block.reshape(key_count, heads, h...]
    all_gather x2, waiting for transfers between devices: 275 us -> 263 us  [side_by_side(): result = lax.all_gather(both, axis, axis=dim, tiled=True)]
    all_to_all x0 -> x1, starting transfers between devices: none -> 8.38 us  [turned_gather(): lax.all_to_all(jnp.stack([both] * lax.axis_size(axis)), axis, 0, 0)]
  transfers between devices with their start and end apart: 4 -> 4, of which waited for: 4 -> 3; matrix products, arithmetic and copies ran while one was open for 9% -> 6% of each run, Pallas kernels for 0% -> 0%
where the time goes in v1:
time: 773 us; the launch traced here: 769 us
  waiting for transfers between devices  304 us (39%)
  other arithmetic  184 us (24%)
  matrix products  110 us (14%)
  blocking collectives  76.6 us (10%)
  local copies, waits for them, and re-layouts  69.4 us (9%)
  between operations  14.4 us (2%)
  starting transfers between devices  8.46 us (1%)
    all_gather x2, waiting for transfers between devices, side_by_side(): result = lax.all_gather(both, axis, axis=dim, tiled=True)  263 us
    another operation x32, other arithmetic  81.2 us
    convert_element_type x16, other arithmetic, stick_block(): jnp.where(visible[None], jnp.exp(jax.nn.log_sigmoid(scores) + between), 0.0)  67.1 us
    dot_general x16, matrix products, stick_block(): jnp.einsum('rhd,khd->hrk', queries, key_block.reshape(key_count, heads, h...  61.5 us
    all_gather x3, blocking collectives, carried_in(): pieces = jax.tree.map(lambda part: lax.all_gather(part, axis), running)  47.7 us
    all_to_all x1, waiting for transfers between devices, turned_gather(): lax.all_to_all(jnp.stack([both] * lax.axis_size(axis)), axis, 0, 0)  41 us
    another operation x16, local copies, waits for them, and re-layouts, stick_block(): lax.cumsum(lost, axis=2, reverse=True) - lost + log_kept[:, :, None]  31 us
    all_to_all x1, blocking collectives, summed_on_arrival(): lax.all_to_all(cut_along(value, dim, length), axis, 0, 0, tiled=True)  28.9 us
  transfers between devices with their start and end apart: 4, of which 3 were waited for; matrix products, arithmetic and copies ran while one was open for 6% of the time, Pallas kernels for 0%

profile of v1, /device:TPU:1, one launch (start us, length us, event | category | flops | bytes accessed | tf_op | source)
XLA Modules:
  0.0 769.5 jit_solution(12442487450140274144)
XLA Ops:
  20.7 130.6 %all-gather.8.cloned.1.call-done = bf16[2048,768]{1,0:T(8,128)(2,1)} async-done(((bf16[32,768]{1,0:T(8,128)(2,1)}), bf16[2048,768]{1,0:T(8,128)(2,1)}) %all-gather.8.cloned.1.call-update) | async-done | bytes 3145744 | tf_op jit(solution)/shard_map/all_gather | solution.py:18
  153.3 19.7 %custom-call.4 = f32[4,1,64,64]{2,3,1,0:T(8,128)S(1)} custom-call(f32[4,1,64,64]{3,2,1,0:T(8,128)S(1)} %fusion.60), custom_call_target="InvertDiagBlocksLowerTriangular" | custom-call | tf_op jit(solution)/shard_map/jit(_solve_triangular)/vmap()/triangular_solve | solution.py:152
  175.8 7.6 while.42
  183.5 9.1 %all-gather = bf16[4,128,128]{2,1,0:T(8,128)(2,1)S(1)} all-gather(bf16[1,128,128]{2,1,0:T(8,128)(2,1)S(1)} %get-tuple-element.235), channel_id=2, replica_groups=mesh['sp_0'=16,'sp_1'=4,'tp'=8] {'sp_1'}, dimensions={0}, use_global_device_ids=true | all-gather | bytes 163840 | tf_op jit(solution)/shard_map/all_gather | solution.py:33
  192.6 9.4 %all-gather.2 = f32[4,128,128]{2,1,0:T(8,128)S(1)} all-gather(f32[1,128,128]{2,1,0:T(8,128)S(1)} %get-tuple-element.236), channel_id=4, replica_groups=mesh['sp_0'=16,'sp_1'=4,'tp'=8] {'sp_1'}, dimensions={0}, use_global_device_ids=true | all-gather | bytes 327680 | tf_op jit(solution)/shard_map/all_gather | solution.py:33
  208.3 8.4 %all-to-all-start = ((bf16[64,32,256]{2,1,0:T(8,128)(2,1)}), bf16[64,32,256]{2,1,0:T(8,128)(2,1)S(1)}, u32[]{:S(2)}, u32[]{:S(2)}) async-start(bf16[64,32,256]{2,1,0:T(8,128)(2,1)} %stack.2), calls=%async_computation | async-start | bytes 2097152 | tf_op jit(solution)/shard_map/all_to_all | solution.py:48
  217.4 41.0 %all-to-all-done = bf16[64,32,256]{2,1,0:T(8,128)(2,1)S(1)} async-done(((bf16[64,32,256]{2,1,0:T(8,128)(2,1)}), bf16[64,32,256]{2,1,0:T(8,128)(2,1)S(1)}, u32[]{:S(2)}, u32[]{:S(2)}) %all-to-all-start) | async-done | bytes 1048608 | tf_op jit(solution)/shard_map/all_to_all | solution.py:48
  261.4 29.3 %all-gather.1 = bf16[2048,128]{1,0:T(8,128)(2,1)S(1)} all-gather(bf16[128,128]{1,0:T(8,128)(2,1)S(1)} %fusion.140), channel_id=3, replica_groups=mesh['sp_0'=16,'sp_1'=4,'tp'=8] {'sp_0'}, dimensions={0}, use_global_device_ids=true | all-gather | bytes 557056 | tf_op jit(solution)/shard_map/all_gather | solution.py:33
  309.0 10.7 %while.41 = (s32[]{:T(128)}, f32[1,128,128]{2,1,0:T(8,128)S(1)}, f32[4,1,64,128]{3,2,1,0:T(8,128)S(1)}, f32[4,1]{0,1:T(1,128)S(1)}, bf16[4,1,64,128]{3,2,1,0:T(8...) while((s32[]{:T(128)}, f32[1,128,128]{2,1,0:T(8,128)S(1)}, ...), condition=%wide.region_14.15_spmd, body=%wide.region_13.14_spmd.sunk | while | flops 7397378 | bytes 510077 | solution.py:275
  320.0 132.8 %all-gather.10.cloned.1.call-done = bf16[16384,256]{0,1:T(8,128)(2,1)} async-done(((bf16[256,256]{0,1:T(8,128)(2,1)}), bf16[16384,256]{0,1:T(8,128)(2,1)}) %all-gather.10.cloned.1.call-update) | async-done | bytes 8388624 | tf_op jit(solution)/shard_map/all_gather | solution.py:18
  452.8 5.8 fusion.199
  458.6 273.0 %while.43 = (s32[]{:T(128)}, f32[2,256,64]{1,2,0:T(8,128)S(1)}, f32[2,256]{1,0:T(2,128)S(1)}, bf16[16384,128]{0,1:T(8,128)(2,1)}, bf16[256,2,64]{0,2,1:T(8,128)(...) while((s32[]{:T(128)}, f32[2,256,64]{1,2,0:T(8,128)S(1)}, ...), condition=%wide.region_6.7_spmd.clone, body=%wide.region_2.6_spmd.clone.sunk | while | flops 215584000 | bytes 44771616 | solution.py:135
  463.9 5.0 fusion.312
  481.0 5.0 fusion.312
  498.0 5.0 fusion.312
  515.1 5.0 fusion.312
  532.2 5.0 fusion.312
  549.2 5.0 fusion.312
  566.3 5.0 fusion.312
  583.4 5.0 fusion.312
  600.4 5.0 fusion.312
  651.6 5.0 fusion.312
  685.7 5.0 fusion.312
  733.3 28.9 %all_to_all.10 = bf16[8,32,2048]{2,1,0:T(8,128)(2,1)S(1)} all-to-all(bf16[8,32,2048]{2,1,0:T(8,128)(2,1)S(1)} %bitcast.319), channel_id=1, replica_groups=mesh['sp_0'=16,'sp_1'=4,'tp'=8] {'tp'}, dimensions={0} | all-to-all | bytes 2097152 | tf_op jit(solution)/shard_map/all_to_all | solution.py:66
  (487 shorter events, 282.8 us)
Async XLA Ops:
  6.5 10.5 %copy-start = (bf16[2048,8]{0,1:T(8,128)(2,1)S(1)}, bf16[2048,8]{0,1:T(8,128)(2,1)}, u32[]{:S(2)}) copy-start(bf16[2048,8]{0,1:T(8,128)(2,1)} %param.33) | copy-start | bytes 98308
  6.5 10.1 %copy-start.3 = (bf16[256,2048]{1,0:T(8,128)(2,1)S(1)}, bf16[256,2048]{1,0:T(8,128)(2,1)}, u32[]{:S(2)}) copy-start(bf16[256,2048]{1,0:T(8,128)(2,1)} %param.24) | copy-start | bytes 3145732
  6.5 10.1 %copy-start.19 = (f32[2048]{0:T(1024)S(1)}, f32[2048]{0:T(1024)}, u32[]{:S(2)}) copy-start(f32[2048]{0:T(1024)} %param.25) | copy-start | bytes 24580
  6.5 144.8 %all-gather.8.cloned.1.call-start = ((), (), s32[]{:S(2)}) async-start(), calls=%async_computation.2 | async-start | bytes 3194880 | tf_op jit(solution)/shard_map/all_gather | solution.py:18
  11.5 281.3 %all-gather.12.cloned.1.call-start = ((), (), s32[]{:S(2)}) async-start(), calls=%async_computation.4 | async-start | bytes 1114112 | tf_op jit(solution)/shard_map/all_gather | solution.py:33
  20.7 153.8 %copy-start.16 = (f32[4,64]{1,0:T(4,128)}, f32[4,64]{1,0:T(4,128)S(1)}, u32[]{:S(2)}) copy-start(f32[4,64]{1,0:T(4,128)S(1)} %get-tuple-element.395) | copy-start | bytes 3076
  183.5 9.1 %copy-start.10 = (bf16[4,1,64,128]{3,2,1,0:T(8,128)(2,1)}, bf16[4,1,64,128]{3,2,1,0:T(8,128)(2,1)S(1)}, u32[]{:S(2)}) copy-start(bf16[4,1,64,128]{3,2,1,0:T(8,128)(2,1)S(1)} %get-tuple-element.672) | copy-start | bytes 196612
  183.5 18.5 %copy-start.24 = (f32[4,1]{0,1:T(1,128)}, f32[4,1]{0,1:T(1,128)S(1)}, u32[]{:S(2)}) copy-start(f32[4,1]{0,1:T(1,128)S(1)} %get-tuple-element.675) | copy-start | bytes 52
  192.6 13.7 %copy-start.6 = (bf16[4,128,128]{2,1,0:T(8,128)(2,1)}, bf16[4,128,128]{2,1,0:T(8,128)(2,1)S(1)}, u32[]{:S(2)}) copy-start(bf16[4,128,128]{2,1,0:T(8,128)(2,1)S(1)} %all-gather) | copy-start | bytes 393220
  202.4 5.9 copy-start.13
  203.2 249.6 %all-gather.10.cloned.1.call-start = ((), (), s32[]{:S(2)}) async-start(), calls=%async_computation.3 | async-start | bytes 8519680 | tf_op jit(solution)/shard_map/all_gather | solution.py:18
  206.3 10.4 %copy-start.28 = (f32[16]{0:T(128)S(1)}, f32[16]{0:T(128)}, u32[]{:S(2)}) copy-start(f32[16]{0:T(128)} %param.34) | copy-start | bytes 196
  208.3 50.1 %all-to-all-start = ((bf16[64,32,256]{2,1,0:T(8,128)(2,1)}), bf16[64,32,256]{2,1,0:T(8,128)(2,1)S(1)}, u32[]{:S(2)}, u32[]{:S(2)}) async-start(bf16[64,32,256]{2,1,0:T(8,128)(2,1)} %stack.2), calls=%async_computation | async-start | bytes 2097152 | tf_op jit(solution)/shard_map/all_to_all | solution.py:48
  292.8 16.0 %copy-start.8 = (f32[128,128]{1,0:T(8,128)S(1)}, f32[128,128]{1,0:T(8,128)}, u32[]{:S(2)}) copy-start(f32[128,128]{1,0:T(8,128)} %convolution_add_fusion.20) | copy-start | bytes 196612
  292.8 16.0 %copy-start.12 = (bf16[128,128]{1,0:T(8,128)(2,1)S(1)}, bf16[128,128]{1,0:T(8,128)(2,1)}, u32[]{:S(2)}) copy-start(bf16[128,128]{1,0:T(8,128)(2,1)} %copy-done.11) | copy-start | bytes 98308
  292.8 16.0 %copy-start.14 = (bf16[128,128]{1,0:T(8,128)(2,1)S(1)}, bf16[128,128]{1,0:T(8,128)(2,1)}, u32[]{:S(2)}) copy-start(bf16[128,128]{1,0:T(8,128)(2,1)} %copy-done.13) | copy-start | bytes 98308
  292.8 16.1 %copy-start.9 = (f32[4,1,64,128]{3,2,1,0:T(8,128)S(1)}, f32[4,1,64,128]{3,2,1,0:T(8,128)}, u32[]{:S(2)}) copy-start(f32[4,1,64,128]{3,2,1,0:T(8,128)} %custom-call.8) | copy-start | bytes 393220
  292.8 16.1 %copy-start.25 = (f32[4,1]{0,1:T(1,128)S(1)}, f32[4,1]{0,1:T(1,128)}, u32[]{:S(2)}) copy-start(f32[4,1]{0,1:T(1,128)} %copy-done.24) | copy-start | bytes 52
  307.6 12.3 %copy-start.23 = (f32[128]{0:T(128)S(1)}, f32[128]{0:T(128)}, u32[]{:S(2)}) copy-start(f32[128]{0:T(128)} %param.39) | copy-start | bytes 1540
  320.0 138.6 %copy-start.18 = (f32[2]{0:T(128)S(1)}, f32[2]{0:T(128)}, u32[]{:S(2)}) copy-start(f32[2]{0:T(128)} %dynamic_slice.62) | copy-start | bytes 28
  458.6 273.1 %copy-start.26 = (f32[64]{0:T(128)S(1)}, f32[64]{0:T(128)}, u32[]{:S(2)}) copy-start(f32[64]{0:T(128)} %param.38) | copy-start | bytes 772
  463.9 5.0 copy-start.1
  481.0 5.0 copy-start.1
  498.0 5.0 copy-start.1
  (39 other events, 125.4 us)
Sparse Core Ops, SparseCore 0:
  11.6 139.7 all-gather.7
  203.3 85.7 all-gather.11
  292.0 160.6 all-gather.9
